TPU v7x, 512 devices: a whole 4x8x8 slice. The times are simulated.
512 devices in a mesh: sp: 64 (over z, y), tp: 8 (over x, core).
Axes of the slice: x: 4, y: 8, z: 8, core: 2. Of those that a mesh axis runs over, the one named last changes fastest.
Arguments:
- tokens_in: bfloat16 [16384, 2048], P('sp', 'tp'), may hold values from -400 to 400
- norm_gain: float32 [2048], replicated, may hold values from 0.1 to 1.9
- w_query: bfloat16 [2048, 1024], P('sp', 'tp'), may hold values from -0.125 to 0.125
- w_forget: bfloat16 [2048, 1024], P('sp', 'tp'), may hold values from -0.125 to 0.125
- w_input: bfloat16 [2048, 1024], P('sp', 'tp'), may hold values from -0.125 to 0.125
- w_rgate: bfloat16 [2048, 1024], P('sp', 'tp'), may hold values from -0.125 to 0.125
- w_pool_in: bfloat16 [2048, 1024], P('sp', 'tp'), may hold values from -0.125 to 0.125
- w_pgate: bfloat16 [2048, 1024], P('sp', 'tp'), may hold values from -0.125 to 0.125
- floor_rate: float32 [1024], P('tp'), as said below
- extra_logdecay: float32 [16384, 8], P('sp', 'tp'), as said below
- state_gain: float32 [1024], P('tp'), may hold values from 0.1 to 1.9
- pool_mix: bfloat16 [8, 128, 128], P('tp'), may hold values from -0.5 to 0.5
- pool_gain: float32 [1024], P('tp'), may hold values from 0.1 to 1.9
- out_rec: bfloat16 [1024, 2048], P('tp', 'sp'), may hold values from -0.125 to 0.125
- out_pool: bfloat16 [1024, 2048], P('tp', 'sp'), may hold values from -0.125 to 0.125
- post_gain: float32 [2048], replicated, may hold values from 0.1 to 1.9
Outputs:
- mixed_out: bfloat16 [16384, 2048], P(('sp', 'tp'))
Inputs may be any that keep to these rules, and one draw needn't show every extreme that they name: `floor_rate`: every entry is positive. `extra_logdecay`: every entry is at most zero.
All inputs are finite; a program needn't handle non-finite values.
Results may differ from a plain program's by a relative error of at most 0.015.
Values may be sent and summed in bfloat16 or wider, within the bound.
A program may use at most 64 MiB of HBM per device.

v0:
```python
import jax
import jax.numpy as jnp
from jax import lax
from jax.sharding import Mesh
from jax.sharding import PartitionSpec as P

DK = 128
BLOCK = 64
SP = ("sp_0", "sp_1")
TP = ("tp_0", "tp_1")
SP_TP = ("sp_0", "sp_1", "tp_0", "tp_1")
eps = 1e-06
coarsest_scale_depth = lax.Precision.HIGHEST


def in_one_piece(arrays, axis, dim, along):
    widths = [a.shape[along] for a in arrays]
    both = jnp.concatenate(arrays, axis=along)
    out = lax.all_gather(both, axis, axis=dim, tiled=True)
    return tuple(jnp.split(out, [sum(widths[:k]) for k in range(1, len(widths))], axis=along))


def cut_rows(length, count):
    turn = length // count
    if turn >= 8:
        turn -= turn % 8
    return [turn * k for k in range(1, count)]


def all_blocks(shard, axes, order):
    tiles = shard[None]
    for k in order:
        tiles = lax.all_gather(tiles, axes[k], axis=0, tiled=True)
    held = [lax.axis_size(axes[k]) for k in reversed(order)]
    tiles = tiles.reshape(*held, *shard.shape)
    turned = sorted(range(len(order)), key=lambda place: order[len(order) - 1 - place])
    return tiles.transpose(*turned, *range(len(order), tiles.ndim)).reshape(-1, *shard.shape)


def joined_along(tiles, dim):
    tiles = jnp.moveaxis(tiles, 0, dim)
    lengths = tiles.shape
    return tiles.reshape(*lengths[:dim], lengths[dim] * lengths[dim + 1], *lengths[dim + 2 :])


def gather_at_once(shard, axes, dim):
    widest = max(range(max(1, shard.ndim - 1)), key=lambda d: shard.shape[d])
    count, done = (len(axes), [])
    for initial, piece in enumerate(
        jnp.split(shard, cut_rows(shard.shape[widest], count), axis=widest)
    ):
        if piece.size:
            order = [(initial - k) % count for k in range(count)]
            done.append(all_blocks(piece, axes, order))
    return joined_along(jnp.concatenate(done, axis=widest + 1), dim)


def nothing_yet(shard, identity):
    return jax.tree.map(
        lambda part, zero: jnp.zeros_like(part) + jnp.asarray(zero, part.dtype), shard, identity
    )


def all_in_one(shard, axis):
    leaves = jax.tree.leaves(shard)
    order = sorted(range(len(leaves)), key=lambda k: -leaves[k].size)
    width = (1, *leaves[order[0]].shape)[-1]
    lines = [
        jnp.pad(leaves[k].reshape(-1), (0, -leaves[k].size % width)).reshape(-1, width)
        for k in order
    ]
    both, at, found = (lax.all_gather(jnp.concatenate(lines), axis), 0, {})
    for k, line in zip(order, lines):
        piece = both[:, at : at + len(line)].reshape(len(both), -1)
        found[k] = piece[:, : leaves[k].size].reshape(-1, *leaves[k].shape)
        at += len(line)
    numbers = iter(range(len(leaves)))
    return jax.tree.map(lambda _: found[next(numbers)], shard)


def prefix_by_axis(shard, axes, combine, identity):
    before = start = nothing_yet(shard, identity)
    so_far = shard
    for axis in reversed(axes):
        peers, index = (lax.axis_size(axis), lax.axis_index(axis))
        pieces = all_in_one(so_far, axis)
        inside, so_far = (start, start)
        for k in range(peers):
            passed = k < index
            so_far = combine(so_far, jax.tree.map(lambda part: part[k], pieces))
            inside = jax.tree.map(lambda new, old: jnp.where(passed, new, old), so_far, inside)
        before = combine(inside, before)
    return before


def shifted(value, axis, steps):
    count = lax.axis_size(axis)
    initial, last = (max(0, -steps), min(count, count - steps))
    return lax.ppermute(value, axis, [(source, source + steps) for source in range(initial, last)])


def gather_turned(arrays, axis, dims):
    turned = [jnp.moveaxis(a, dim, 0) for a, dim in zip(arrays, dims)]
    widths = [t[0].size for t in turned]
    both = jnp.concatenate([t.reshape(-1, w) for t, w in zip(turned, widths)], axis=1)
    out = lax.all_gather(both, axis, axis=0, tiled=True)
    tiles = jnp.split(out, [sum(widths[:k]) for k in range(1, len(widths))], axis=1)
    return tuple(
        (
            jnp.moveaxis(b.reshape(-1, *t.shape[1:]), 0, dim)
            for b, t, dim in zip(tiles, turned, dims)
        )
    )


def chain_merge(earlier, later):
    return (earlier[0] * later[0], later[0][..., None] * earlier[1] + later[1])


def local_blocks(qs, keys, values, logs):
    causal = jnp.arange(BLOCK)[:, None] >= jnp.arange(BLOCK)[None, :]
    heads_dev = qs.shape[1]

    def advance(carry, member):
        carried_memory_matrix, start = carry
        probe_segment, key_piece, input_piece, gc = member
        prefix_sum_vector = jnp.cumsum(gc, axis=1)
        last_index = prefix_sum_vector[:, -1]
        cross_segment_contribution = jnp.einsum(
            "abz,azy->aby",
            probe_segment * jnp.exp(prefix_sum_vector),
            carried_memory_matrix,
            precision=coarsest_scale_depth,
        )
        diff = prefix_sum_vector[:, :, None, :] - prefix_sum_vector[:, None, :, :]
        weight = jnp.where(causal[None, :, :, None], jnp.exp(jnp.minimum(diff, 0.0)), 0.0)
        scores = jnp.einsum(
            "htk,hsk,htsk->hts", probe_segment, key_piece, weight, precision=coarsest_scale_depth
        )
        final_result = cross_segment_contribution + jnp.einsum(
            "hts,hsv->htv", scores, input_piece, precision=coarsest_scale_depth
        )
        carried_memory_matrix = jnp.exp(last_index)[..., None] * carried_memory_matrix + jnp.einsum(
            "njp,njq->npq",
            key_piece * jnp.exp(last_index[:, None, :] - prefix_sum_vector),
            input_piece,
            precision=coarsest_scale_depth,
        )
        pool_reach = probe_segment * jnp.exp(start[:, None, :] + prefix_sum_vector)
        return ((carried_memory_matrix, start + last_index), (final_result, pool_reach))

    begin = (jnp.zeros((heads_dev, DK, DK), jnp.float32), jnp.zeros((heads_dev, DK), jnp.float32))
    (carried_memory_matrix, total), (final_result, pool_reach) = lax.scan(
        advance, begin, (qs, keys, values, logs)
    )
    return (carried_memory_matrix, total, final_result, pool_reach)


def per_device(
    tokens_in,
    norm_gain,
    w_query,
    w_forget,
    w_input,
    w_rgate,
    w_pool_in,
    w_pgate,
    floor_rate,
    extra_logdecay,
    state_gain,
    pool_mix,
    pool_gain,
    out_rec,
    out_pool,
    post_gain,
):
    gathered = in_one_piece((w_query, w_forget, w_input, w_rgate, w_pool_in, w_pgate), SP, 0, 1)
    joined = jnp.concatenate(gathered, axis=1)
    head_cols = w_query.shape[1]
    positions = tokens_in.shape[0]
    model_width = norm_gain.shape[0]
    wide = gather_at_once(tokens_in, TP, 1).astype(jnp.float32)
    scaled = (wide * norm_gain[None, :]).astype(jnp.bfloat16)
    totals = jnp.dot(scaled, joined, preferred_element_type=jnp.float32)
    squares = jnp.sum(wide * wide, axis=1)
    inv_rms = lax.rsqrt(squares / model_width + eps)
    proj = (totals * inv_rms[:, None]).astype(jnp.bfloat16)
    query = proj[:, 0:head_cols]
    forget = proj[:, head_cols : 2 * head_cols]
    inputs = proj[:, 2 * head_cols : 3 * head_cols]
    rgate = proj[:, 3 * head_cols : 4 * head_cols]
    pool_in = proj[:, 4 * head_cols : 5 * head_cols]
    pgate = proj[:, 5 * head_cols : 6 * head_cols]
    heads_dev = head_cols // DK
    blocks = positions // BLOCK

    def to_blocks(array):
        return array.reshape(blocks, BLOCK, heads_dev, DK).transpose(0, 2, 1, 3)

    forget32 = forget.astype(jnp.float32)
    key_gate = -jnp.expm1(-floor_rate)[None, :] * jax.nn.sigmoid(-forget32)
    log_forget = jnp.log1p(-key_gate) + jnp.repeat(extra_logdecay, DK, axis=1)
    qs = query.astype(jnp.float32) * DK ** (-0.5)
    carried_memory_matrix, total, final_result, pool_reach = local_blocks(
        to_blocks(qs),
        to_blocks(key_gate),
        to_blocks(inputs.astype(jnp.float32)),
        to_blocks(log_forget),
    )
    decays = jnp.exp(total)
    tail_rows = pool_in[positions - 16 :]
    carried = prefix_by_axis(
        (decays, carried_memory_matrix),
        SP,
        chain_merge,
        (jnp.ones_like(decays), jnp.zeros_like(carried_memory_matrix)),
    )
    incoming_state = carried[1]
    previous = shifted(tail_rows, SP, 1).astype(jnp.float32)
    recurrent_output = final_result + jnp.einsum(
        "izaf,zfu->izau", pool_reach, incoming_state, precision=coarsest_scale_depth
    )
    grouped = recurrent_output.transpose(0, 2, 1, 3).reshape(positions, heads_dev, DK)
    normed = grouped * lax.rsqrt(jnp.mean(grouped * grouped, axis=2, keepdims=True) + eps)
    y_rec = (
        normed.reshape(positions, head_cols)
        * state_gain[None, :]
        * jax.nn.silu(rgate.astype(jnp.float32))
    ).astype(jnp.bfloat16)
    group = lax.axis_index(TP) * heads_dev + jnp.arange(head_cols) // DK
    window = jnp.power(2, 1 + group % 4).astype(jnp.int32)
    pool32 = pool_in.astype(jnp.float32)
    extended = jnp.concatenate([previous, pool32], axis=0)
    summed_rows = jnp.zeros((positions, head_cols), jnp.float32)
    for offset in range(16):
        rows_back = extended[16 - offset : 16 - offset + positions]
        summed_rows = summed_rows + jnp.where((offset < window)[None, :], rows_back, 0.0)
    place = lax.axis_index(SP) * positions + jnp.arange(positions)
    count = jnp.minimum(place[:, None] + 1, window[None, :]).astype(jnp.float32)
    mixed = (summed_rows / count - pool32).astype(jnp.bfloat16)
    mapped = jnp.einsum(
        "tgc,gcd->tgd",
        mixed.reshape(positions, heads_dev, DK),
        pool_mix,
        preferred_element_type=jnp.float32,
    ).reshape(positions, head_cols)
    y_pool = (mapped * pool_gain[None, :] * jax.nn.silu(pgate.astype(jnp.float32))).astype(
        jnp.bfloat16
    )
    out_parts = gather_turned((out_rec, out_pool), SP, (1, 1))
    both = jnp.concatenate([y_rec, y_pool], axis=1)
    weight_cat = jnp.concatenate(out_parts, axis=0)
    groups = lax.axis_size(TP)
    exchanged = lax.all_to_all(both, TP, split_axis=0, concat_axis=1, tiled=True)
    whole = lax.all_gather(weight_cat, TP, axis=0, tiled=True)
    owned = exchanged.shape[0]
    terms = jnp.einsum(
        "tjc,jcd->jtd",
        exchanged.reshape(owned, groups, 2 * head_cols),
        whole.reshape(groups, 2 * head_cols, model_width),
        preferred_element_type=jnp.float32,
    )
    summed = jnp.sum(terms.astype(jnp.bfloat16).astype(jnp.float32), axis=0)
    final = (
        summed
        * lax.rsqrt(jnp.mean(summed * summed, axis=1, keepdims=True) + eps)
        * post_gain[None, :]
    )
    return final.astype(jnp.bfloat16)


def solution(mesh):
    torus = Mesh(mesh.devices.reshape(8, 8, 4, 2), ("sp_0", "sp_1", "tp_0", "tp_1"))
    return jax.shard_map(
        per_device,
        mesh=torus,
        in_specs=(
            P(SP, TP),
            P(),
            P(SP, TP),
            P(SP, TP),
            P(SP, TP),
            P(SP, TP),
            P(SP, TP),
            P(SP, TP),
            P(TP),
            P(SP, TP),
            P(TP),
            P(TP, None, None),
            P(TP),
            P(TP, SP),
            P(TP, SP),
            P(),
        ),
        out_specs=P(SP_TP, None),
        check_vma=False,
    )
```

profile of v0, /device:TPU:1, one launch (start us, length us, event | category | flops | bytes accessed | tf_op | source)
XLA Modules:
  0.0 284.9 jit_solution(16253742989583789362)
XLA Ops:
  6.5 1.3 pad_maximum_fusion.4
  12.9 0.9 fusion.167
  13.7 10.5 %all-gather = bf16[512,256]{1,0:T(8,128)(2,1)S(1)} all-gather(bf16[128,256]{1,0:T(8,128)(2,1)S(1)} %get-tuple-element.199), channel_id=2, replica_groups=mesh['sp_0'=8,'sp_1'=8,'tp_0'=4,'tp_1'=2] {'tp_0'}, dimensions={0}, use_global_device_ids=true | all-gather | bytes 327680 | tf_op jit(solution)/shard_map/all_gather | solution.py:33
  24.3 10.4 %all_gather.34 = bf16[8,128,256]{2,1,0:T(8,128)(2,1)S(1)} all-gather(bf16[4,128,256]{2,1,0:T(8,128)(2,1)S(1)} %bitcast.247), channel_id=1, replica_groups=mesh['sp_0'=8,'sp_1'=8,'tp_0'=4,'tp_1'=2] {'tp_1'}, dimensions={0}, use_global_device_ids=true | all-gather | bytes 786432 | tf_op jit(solution)/shard_map/all_gather | solution.py:33
  34.7 1.9 all-gather.1
  36.8 10.3 %all_gather.36 = bf16[8,128,256]{2,1,0:T(8,128)(2,1)S(1)} all-gather(bf16[2,128,256]{2,1,0:T(8,128)(2,1)S(1)} %bitcast.249), channel_id=1, replica_groups=mesh['sp_0'=8,'sp_1'=8,'tp_0'=4,'tp_1'=2] {'tp_0'}, dimensions={0}, use_global_device_ids=true | all-gather | bytes 655360 | tf_op jit(solution)/shard_map/all_gather | solution.py:33
  47.2 46.0 %all-gather.12.cloned.1.call-done = bf16[2048,256]{1,0:T(8,128)(2,1)} async-done(((bf16[32,256]{1,0:T(8,128)(2,1)}), bf16[2048,256]{1,0:T(8,128)(2,1)}) %all-gather.12.cloned.1.call-update) | async-done | bytes 1048592 | tf_op jit(solution)/shard_map/all_gather | solution.py:106
  93.2 1.3 slice_bitcast_fusion.2
  94.5 1.1 pad_maximum_fusion.1
  96.0 1.9 copy.67
  98.1 1.9 fusion.36
  100.0 79.3 %all-gather.10.cloned.1.call-done = bf16[2048,768]{1,0:T(8,128)(2,1)} async-done(((bf16[32,768]{1,0:T(8,128)(2,1)}), bf16[2048,768]{1,0:T(8,128)(2,1)}) %all-gather.10.cloned.1.call-update) | async-done | bytes 3145744 | tf_op jit(solution)/shard_map/all_gather | solution.py:19
  179.3 2.9 %fusion.38 = bf16[256,768]{1,0:T(8,128)(2,1)S(1)} fusion(bf16[256,2048]{0,1:T(8,128)(2,1)S(1)} %fusion.36, bf16[2048,768]{1,0:T(8,128)(2,1)} %all-gather.10.cloned.1.call-done, f32[256]{0:T(256)S(1)} %add_rsqrt_fusion.1), kind=kOutput, calls=%fused_computation.54 | convolution fusion | flops 805699584 | bytes 4588544 | tf_op jit(solution)/shard_map/dot_general | solution.py:184
  182.3 2.7 collective-permute-start
  185.1 13.2 %while.17 = (s32[]{:T(128)}, f32[1,128,128]{2,1,0:T(8,128)S(1)}, f32[1,128]{1,0:T(1,128)S(1)}, f32[4,1,64,128]{3,2,1,0:T(8,128)S(1)}, f32[4,1,64,128]{3,2,1,0:T(...) while((s32[]{:T(128)}, f32[1,128,128]{2,1,0:T(8,128)S(1)}, ...), condition=%wide.region_3.4_spmd.clone, body=%wide.region_1.3_spmd.clone.sunk | while | flops 35234048 | bytes 5177500 | solution.py:153
  186.5 1.7 fusion.196
  189.8 1.7 fusion.196
  193.1 1.7 fusion.196
  196.4 1.7 fusion.196
  198.4 22.0 %all-gather.4 = f32[8,129,128]{2,1,0:T(8,128)S(1)} all-gather(f32[1,129,128]{2,1,0:T(8,128)S(1)} %maximum_bitcast_fusion), channel_id=4, replica_groups=mesh['sp_0'=8,'sp_1'=8,'tp_0'=4,'tp_1'=2] {'sp_1'}, dimensions={0}, use_global_device_ids=true | all-gather | bytes 594432 | tf_op jit(solution)/shard_map/all_gather | solution.py:72
  220.6 21.3 %all-gather.5 = f32[8,129,128]{2,1,0:T(8,128)S(1)} all-gather(f32[1,129,128]{2,1,0:T(8,128)S(1)} %maximum_bitcast_fusion.1), channel_id=5, replica_groups=mesh['sp_0'=8,'sp_1'=8,'tp_0'=4,'tp_1'=2] {'sp_0'}, dimensions={0}, use_global_device_ids=true | all-gather | bytes 594432 | tf_op jit(solution)/shard_map/all_gather | solution.py:72
  244.0 16.6 %all-to-all-start = ((bf16[8,32,256]{2,1,0:T(8,128)(2,1)}), bf16[8,32,256]{2,1,0:T(8,128)(2,1)S(1)}, u32[]{:S(2)}, u32[]{:S(2)}) async-start(bf16[8,32,256]{2,1,0:T(8,128)(2,1)} %bitcast.46), calls=%async_computation | async-start | bytes 262144 | tf_op jit(solution)/shard_map/all_to_all | solution.py:254
  260.6 11.9 %copy.74 = bf16[2048,2048]{1,0:T(8,128)(2,1)} copy(bf16[2048,2048]{0,1:T(8,128)(2,1)} %all-gather.14.cloned.1.call-done) | data formatting | bytes 16777216 | tf_op jit(solution)/shard_map/all_gather | solution.py:255
  272.5 4.9 %fusion.37 = f32[32,2048]{1,0:T(8,128)S(1)} fusion(bf16[8,256,2048]{2,1,0:T(8,128)(2,1)} %bitcast.239, bf16[8,32,256]{2,1,0:T(8,128)(2,1)S(1)} %all-to-all-done), kind=kOutput, calls=%fused_computation.52 | convolution fusion | flops 269942784 | bytes 8781824 | tf_op jit(solution)/shard_map/tjc,jcd->jtd/dot_general | solution.py:257
  (119 shorter events, 15.0 us)
Async XLA Ops:
  6.5 236.3 %copy-start = (bf16[1,128,128]{2,1,0:T(8,128)(2,1)S(1)}, bf16[1,128,128]{2,1,0:T(8,128)(2,1)}, u32[]{:S(2)}) copy-start(bf16[1,128,128]{2,1,0:T(8,128)(2,1)} %param.29) | copy-start | bytes 98308
  6.5 86.7 %all-gather.12.cloned.1.call-start = ((), (), s32[]{:S(2)}) async-start(), calls=%async_computation.2 | async-start | bytes 1064960 | tf_op jit(solution)/shard_map/all_gather | solution.py:106
  7.9 171.4 %all-gather.10.cloned.1.call-start = ((), (), s32[]{:S(2)}) async-start(), calls=%async_computation.1 | async-start | bytes 3194880 | tf_op jit(solution)/shard_map/all_gather | solution.py:19
  12.2 0.6 copy-start.1
  12.8 247.8 %all-gather.14.cloned.1.call-start = ((), (), s32[]{:S(2)}) async-start(), calls=%async_computation.3 | async-start | bytes 9437184 | tf_op jit(solution)/shard_map/all_gather | solution.py:255
  96.0 2.1 copy-start.6
  96.0 2.1 copy-start.2
  100.0 85.0 %copy-start.4 = (f32[256,1]{0,1:T(1,128)S(1)}, f32[256,1]{0,1:T(1,128)}, u32[]{:S(2)}) copy-start(f32[256,1]{0,1:T(1,128)} %param.27) | copy-start | bytes 3076
  182.3 60.6 %collective-permute-start = (bf16[16,128]{1,0:T(8,128)(2,1)S(1)}, bf16[16,128]{1,0:T(8,128)(2,1)S(1)}, u32[]{:S(2)}, u32[]{:S(2)}) collective-permute-start(bf16[16,128]{1,0:T(8,128)(2,1)S(1)} %slice.312), channel_id=1, source_target_pairs={{0,8},{8,16},{16,24},{24,32},{32,40},{40,48},{48,56},{56,64},{64,7... | collective-permute-start | bytes 12296 | tf_op jit(solution)/shard_map/ppermute | solution.py:99
  198.3 44.4 %copy-start.5 = (f32[128]{0:T(128)S(1)}, f32[128]{0:T(128)}, u32[]{:S(2)}) copy-start(f32[128]{0:T(128)} %param.28) | copy-start | bytes 1540
  198.3 44.5 %copy-start.7 = (f32[128]{0:T(128)S(1)}, f32[128]{0:T(128)}, u32[]{:S(2)}) copy-start(f32[128]{0:T(128)} %param.30) | copy-start | bytes 1540
  244.0 28.5 %all-to-all-start = ((bf16[8,32,256]{2,1,0:T(8,128)(2,1)}), bf16[8,32,256]{2,1,0:T(8,128)(2,1)S(1)}, u32[]{:S(2)}, u32[]{:S(2)}) async-start(bf16[8,32,256]{2,1,0:T(8,128)(2,1)} %bitcast.46), calls=%async_computation | async-start | bytes 262144 | tf_op jit(solution)/shard_map/all_to_all | solution.py:254
  272.5 5.1 %copy-start.3 = (f32[2048]{0:T(1024)S(1)}, f32[2048]{0:T(1024)}, u32[]{:S(2)}) copy-start(f32[2048]{0:T(1024)} %param.33) | copy-start | bytes 24580
Sparse Core Ops, SparseCore 0:
  10.4 82.7 all-gather.11
  96.2 83.0 all-gather.9
  181.5 59.5 all-gather.13
where the time goes:
time: 286 us; the launch traced here: 285 us
  waiting for transfers between devices  125 us (44%)
  blocking collectives  76.4 us (27%)
  local copies, waits for them, and re-layouts  21.1 us (7%)
  starting transfers between devices  19.4 us (7%)
  other arithmetic  16.9 us (6%)
  between operations  13.5 us (5%)
  matrix products  11.8 us (4%)
    all_gather x1, waiting for transfers between devices, in_one_piece(): out = lax.all_gather(both, axis, axis=dim, tiled=True)  79.3 us
    all_gather x1, waiting for transfers between devices, gather_turned(): out = lax.all_gather(both, axis, axis=0, tiled=True)  46 us
    all_gather x2, blocking collectives, all_in_one(): both, at, found = (lax.all_gather(jnp.concatenate(lines), axis), 0, {})  43.3 us
    all_gather x4, blocking collectives, all_blocks(): tiles = lax.all_gather(tiles, axes[k], axis=0, tiled=True)  33.1 us
    all_to_all x1, starting transfers between devices, per_device(): lax.all_to_all(both, TP, split_axis=0, concat_axis=1, tiled=True)  16.6 us
    all_gather x1, local copies, waits for them, and re-layouts, per_device(): whole = lax.all_gather(weight_cat, TP, axis=0, tiled=True)  11.9 us
    dot_general x4, other arithmetic, advance(): jnp.einsum('htk,hsk,htsk->hts', probe_segment, key_piece, weight, precisi...  6.81 us
  transfers between devices with their start and end apart: 5, of which 2 were waited for; matrix products, arithmetic and copies ran while one was open for 15% of the time, Pallas kernels for 0%

commit v1 on v0

--- a/solution.py
+++ b/solution.py
@@ -174,6 +174,13 @@
     out_pool,
     post_gain,
 ):
+
+    def process_the_zones(point, at_axis, d_out):
+        placed = jnp.split(point, lax.axis_size(TP), at_axis)
+        reached = lax.all_to_all(jnp.stack(placed, 0), axis_name=TP, split_axis=0, concat_axis=0)
+        t1 = jnp.concatenate(reached, d_out)
+        return t1
+
     gathered = in_one_piece((w_query, w_forget, w_input, w_rgate, w_pool_in, w_pgate), SP, 0, 1)
     joined = jnp.concatenate(gathered, axis=1)
     head_cols = w_query.shape[1]
@@ -251,7 +258,7 @@
     both = jnp.concatenate([y_rec, y_pool], axis=1)
     weight_cat = jnp.concatenate(out_parts, axis=0)
     groups = lax.axis_size(TP)
-    exchanged = lax.all_to_all(both, TP, split_axis=0, concat_axis=1, tiled=True)
+    exchanged = process_the_zones(both, 0, 1)
     whole = lax.all_gather(weight_cat, TP, axis=0, tiled=True)
     owned = exchanged.shape[0]
     terms = jnp.einsum(

time: 286 us -> 290 us (1.014)
  other arithmetic: 16.9 us -> 21.1 us
    unnamed x5 -> x12, other arithmetic: 0.03 us -> 4.29 us
  transfers between devices with their start and end apart: 5 -> 5, of which waited for: 2 -> 2; matrix products, arithmetic and copies ran while one was open for 15% -> 16% of each run, Pallas kernels for 0% -> 0%
where the time goes in v1:
time: 290 us; the launch traced here: 289 us
  waiting for transfers between devices  125 us (43%)
  blocking collectives  76.4 us (26%)
  local copies, waits for them, and re-layouts  21.1 us (7%)
  other arithmetic  21.1 us (7%)
  starting transfers between devices  19.4 us (7%)
  between operations  13.5 us (5%)
  matrix products  11.8 us (4%)
    all_gather x1, waiting for transfers between devices, in_one_piece(): out = lax.all_gather(both, axis, axis=dim, tiled=True)  79.7 us
    all_gather x1, waiting for transfers between devices, gather_turned(): out = lax.all_gather(both, axis, axis=0, tiled=True)  45.6 us
    all_gather x2, blocking collectives, all_in_one(): both, at, found = (lax.all_gather(jnp.concatenate(lines), axis), 0, {})  43.3 us
    all_gather x4, blocking collectives, all_blocks(): tiles = lax.all_gather(tiles, axes[k], axis=0, tiled=True)  33.1 us
    all_to_all x1, starting transfers between devices, process_the_zones(): lax.all_to_all(jnp.stack(placed, 0), axis_name=TP, split_axis=0, concat_a...  16.6 us
    all_gather x1, local copies, waits for them, and re-layouts, per_device(): whole = lax.all_gather(weight_cat, TP, axis=0, tiled=True)  11.9 us
    dot_general x4, other arithmetic, advance(): jnp.einsum('htk,hsk,htsk->hts', probe_segment, key_piece, weight, precisi...  6.81 us
  transfers between devices with their start and end apart: 5, of which 2 were waited for; matrix products, arithmetic and copies ran while one was open for 16% of the time, Pallas kernels for 0%

profile of v1, /device:TPU:1, one launch (start us, length us, event | category | flops | bytes accessed | tf_op | source)
XLA Modules:
  0.0 289.1 jit_solution(1886598099277732226)
XLA Ops:
  6.5 1.3 pad_maximum_fusion.4
  12.9 0.9 fusion.175
  13.7 10.5 %all-gather = bf16[512,256]{1,0:T(8,128)(2,1)S(1)} all-gather(bf16[128,256]{1,0:T(8,128)(2,1)S(1)} %get-tuple-element.199), channel_id=2, replica_groups=mesh['sp_0'=8,'sp_1'=8,'tp_0'=4,'tp_1'=2] {'tp_0'}, dimensions={0}, use_global_device_ids=true | all-gather | bytes 327680 | tf_op jit(solution)/shard_map/all_gather | solution.py:33
  24.3 10.4 %all_gather.34 = bf16[8,128,256]{2,1,0:T(8,128)(2,1)S(1)} all-gather(bf16[4,128,256]{2,1,0:T(8,128)(2,1)S(1)} %bitcast.264), channel_id=1, replica_groups=mesh['sp_0'=8,'sp_1'=8,'tp_0'=4,'tp_1'=2] {'tp_1'}, dimensions={0}, use_global_device_ids=true | all-gather | bytes 786432 | tf_op jit(solution)/shard_map/all_gather | solution.py:33
  34.7 1.9 all-gather.1
  36.6 10.3 %all_gather.36 = bf16[8,128,256]{2,1,0:T(8,128)(2,1)S(1)} all-gather(bf16[2,128,256]{2,1,0:T(8,128)(2,1)S(1)} %bitcast.266), channel_id=1, replica_groups=mesh['sp_0'=8,'sp_1'=8,'tp_0'=4,'tp_1'=2] {'tp_0'}, dimensions={0}, use_global_device_ids=true | all-gather | bytes 655360 | tf_op jit(solution)/shard_map/all_gather | solution.py:33
  47.6 45.6 %all-gather.12.cloned.1.call-done = bf16[2048,256]{1,0:T(8,128)(2,1)} async-done(((bf16[32,256]{1,0:T(8,128)(2,1)}), bf16[2048,256]{1,0:T(8,128)(2,1)}) %all-gather.12.cloned.1.call-update) | async-done | bytes 1048592 | tf_op jit(solution)/shard_map/all_gather | solution.py:106
  93.2 1.3 slice_bitcast_fusion.2
  94.5 1.1 pad_maximum_fusion.1
  95.7 1.9 copy.67
  97.7 1.9 fusion.36
  99.6 79.7 %all-gather.10.cloned.1.call-done = bf16[2048,768]{1,0:T(8,128)(2,1)} async-done(((bf16[32,768]{1,0:T(8,128)(2,1)}), bf16[2048,768]{1,0:T(8,128)(2,1)}) %all-gather.10.cloned.1.call-update) | async-done | bytes 3145744 | tf_op jit(solution)/shard_map/all_gather | solution.py:19
  179.3 2.9 %fusion.38 = bf16[256,768]{1,0:T(8,128)(2,1)S(1)} fusion(bf16[256,2048]{0,1:T(8,128)(2,1)S(1)} %fusion.36, bf16[2048,768]{1,0:T(8,128)(2,1)} %all-gather.10.cloned.1.call-done, f32[256]{0:T(256)S(1)} %add_rsqrt_fusion.1), kind=kOutput, calls=%fused_computation.54 | convolution fusion | flops 805699584 | bytes 4588544 | tf_op jit(solution)/shard_map/dot_general | solution.py:191
  182.3 2.7 collective-permute-start
  185.1 13.2 %while.17 = (s32[]{:T(128)}, f32[1,128,128]{2,1,0:T(8,128)S(1)}, f32[1,128]{1,0:T(1,128)S(1)}, f32[4,1,64,128]{3,2,1,0:T(8,128)S(1)}, f32[4,1,64,128]{3,2,1,0:T(...) while((s32[]{:T(128)}, f32[1,128,128]{2,1,0:T(8,128)S(1)}, ...), condition=%wide.region_3.4_spmd.clone, body=%wide.region_1.3_spmd.clone.sunk | while | flops 35234048 | bytes 5177500 | solution.py:153
  186.5 1.7 fusion.204
  189.8 1.7 fusion.204
  193.1 1.7 fusion.204
  196.4 1.7 fusion.204
  198.4 22.0 %all-gather.4 = f32[8,129,128]{2,1,0:T(8,128)S(1)} all-gather(f32[1,129,128]{2,1,0:T(8,128)S(1)} %maximum_bitcast_fusion), channel_id=4, replica_groups=mesh['sp_0'=8,'sp_1'=8,'tp_0'=4,'tp_1'=2] {'sp_1'}, dimensions={0}, use_global_device_ids=true | all-gather | bytes 594432 | tf_op jit(solution)/shard_map/all_gather | solution.py:72
  220.6 21.3 %all-gather.5 = f32[8,129,128]{2,1,0:T(8,128)S(1)} all-gather(f32[1,129,128]{2,1,0:T(8,128)S(1)} %maximum_bitcast_fusion.1), channel_id=5, replica_groups=mesh['sp_0'=8,'sp_1'=8,'tp_0'=4,'tp_1'=2] {'sp_0'}, dimensions={0}, use_global_device_ids=true | all-gather | bytes 594432 | tf_op jit(solution)/shard_map/all_gather | solution.py:72
  248.2 16.6 %all-to-all-start = ((bf16[8,32,256]{2,1,0:T(8,128)(2,1)}), bf16[8,32,256]{2,1,0:T(8,128)(2,1)S(1)}, u32[]{:S(2)}, u32[]{:S(2)}) async-start(bf16[8,32,256]{2,1,0:T(8,128)(2,1)} %constant_dynamic-update-slice_fusion.6), calls=%async_computation | async-start | bytes 262144 | tf_op jit(solution)/shard_map/all_to_all | solution.py:180
  264.8 11.9 %copy.74 = bf16[2048,2048]{1,0:T(8,128)(2,1)} copy(bf16[2048,2048]{0,1:T(8,128)(2,1)} %all-gather.14.cloned.1.call-done) | data formatting | bytes 16777216 | tf_op jit(solution)/shard_map/all_gather | solution.py:262
  276.7 4.9 %fusion.37 = f32[32,2048]{1,0:T(8,128)S(1)} fusion(bf16[8,256,2048]{2,1,0:T(8,128)(2,1)} %bitcast.256, bf16[8,32,256]{2,1,0:T(8,128)(2,1)S(1)} %all-to-all-done), kind=kOutput, calls=%fused_computation.52 | convolution fusion | flops 269942784 | bytes 8781824 | tf_op jit(solution)/shard_map/tjc,jcd->jtd/dot_general | solution.py:264
  (126 shorter events, 19.2 us)
Async XLA Ops:
  6.5 236.3 %copy-start = (bf16[1,128,128]{2,1,0:T(8,128)(2,1)S(1)}, bf16[1,128,128]{2,1,0:T(8,128)(2,1)}, u32[]{:S(2)}) copy-start(bf16[1,128,128]{2,1,0:T(8,128)(2,1)} %param.29) | copy-start | bytes 98308
  6.5 86.7 %all-gather.12.cloned.1.call-start = ((), (), s32[]{:S(2)}) async-start(), calls=%async_computation.2 | async-start | bytes 1064960 | tf_op jit(solution)/shard_map/all_gather | solution.py:106
  7.9 171.4 %all-gather.10.cloned.1.call-start = ((), (), s32[]{:S(2)}) async-start(), calls=%async_computation.1 | async-start | bytes 3194880 | tf_op jit(solution)/shard_map/all_gather | solution.py:19
  12.2 0.6 copy-start.1
  12.8 252.0 %all-gather.14.cloned.1.call-start = ((), (), s32[]{:S(2)}) async-start(), calls=%async_computation.3 | async-start | bytes 9437184 | tf_op jit(solution)/shard_map/all_gather | solution.py:262
  46.9 0.7 copy-start.6
  95.7 2.0 copy-start.2
  99.6 85.4 %copy-start.4 = (f32[256,1]{0,1:T(1,128)S(1)}, f32[256,1]{0,1:T(1,128)}, u32[]{:S(2)}) copy-start(f32[256,1]{0,1:T(1,128)} %param.27) | copy-start | bytes 3076
  182.3 60.6 %collective-permute-start = (bf16[16,128]{1,0:T(8,128)(2,1)S(1)}, bf16[16,128]{1,0:T(8,128)(2,1)S(1)}, u32[]{:S(2)}, u32[]{:S(2)}) collective-permute-start(bf16[16,128]{1,0:T(8,128)(2,1)S(1)} %slice.312), channel_id=1, source_target_pairs={{0,8},{8,16},{16,24},{24,32},{32,40},{40,48},{48,56},{56,64},{64,7... | collective-permute-start | bytes 12296 | tf_op jit(solution)/shard_map/ppermute | solution.py:99
  198.3 44.4 %copy-start.5 = (f32[128]{0:T(128)S(1)}, f32[128]{0:T(128)}, u32[]{:S(2)}) copy-start(f32[128]{0:T(128)} %param.28) | copy-start | bytes 1540
  198.3 44.5 %copy-start.7 = (f32[128]{0:T(128)S(1)}, f32[128]{0:T(128)}, u32[]{:S(2)}) copy-start(f32[128]{0:T(128)} %param.30) | copy-start | bytes 1540
  248.2 28.5 %all-to-all-start = ((bf16[8,32,256]{2,1,0:T(8,128)(2,1)}), bf16[8,32,256]{2,1,0:T(8,128)(2,1)S(1)}, u32[]{:S(2)}, u32[]{:S(2)}) async-start(bf16[8,32,256]{2,1,0:T(8,128)(2,1)} %constant_dynamic-update-slice_fusion.6), calls=%async_computation | async-start | bytes 262144 | tf_op jit(solution)/shard_map/all_to_all | solution.py:180
  276.7 5.1 %copy-start.3 = (f32[2048]{0:T(1024)S(1)}, f32[2048]{0:T(1024)}, u32[]{:S(2)}) copy-start(f32[2048]{0:T(1024)} %param.33) | copy-start | bytes 24580
Sparse Core Ops, SparseCore 0:
  10.4 82.7 all-gather.11
  96.2 83.0 all-gather.9
  181.5 59.5 all-gather.13
